TPU v7x, 256 devices: a 4x2x16 block of a 4x16x16 slice. The times are simulated.
256 devices in a mesh: grp: 2 (over y), fs: 16 (over z), tp: 8 (over x, core).
Axes of the slice: x: 4, y: 2, z: 16, core: 2. Of those that a mesh axis runs over, the one named last changes fastest.
The devices are a block of a 4x16x16 slice.
Arguments:
- tokens: bfloat16 [32768, 2048], P(('grp', 'fs', 'tp')), parts along dimension 0, may hold values from -12 to 12
- norm_gain: float32 [2048], replicated, may hold values from 0.1 to 1.9
- w_in: bfloat16 [2048, 8192], P('fs', 'tp'), may hold values from -0.125 to 0.125
- w_out: bfloat16 [8192, 2048], P('tp', 'fs'), may hold values from -0.0625 to 0.0625
Outputs:
- mixed: bfloat16 [32768, 2048], P(('grp', 'fs', 'tp')), parts along dimension 0
There are 2 independent parts, one for each index of `grp`. A program takes and returns all parts, laid end to end along the dimension named above; an argument that names none is the same for every part. Nothing has to cross between parts.
All inputs are finite; a program needn't handle non-finite values.
Results may differ from a plain program's by a relative error of at most 0.012.
Values may be sent and summed in bfloat16 or wider, within the bound.
No kernel may reach another device: no remote copies, remote signals or barrier semaphores. Data moves between devices by JAX's collectives and lax.ppermute only.
A program may use at most 64 MiB of HBM per device.

v0:
```python
import jax
import jax.numpy as jnp
from jax import lax
from jax.sharding import PartitionSpec as P

EPS = 1e-06


def from_everyone(shard, axis):
    copies = jnp.broadcast_to(shard, (lax.axis_size(axis), *shard.shape))
    return lax.all_to_all(copies, axis, split_axis=0, concat_axis=0, tiled=True)


def joined_along(parts, dim):
    parts = jnp.moveaxis(parts, 0, dim)
    shape = parts.shape
    return parts.reshape(*shape[:dim], shape[dim] * shape[dim + 1], *shape[dim + 2 :])


def collect(shard, axis, dim):
    parts = from_everyone(shard, axis)
    return joined_along(parts, dim)


def local(tokens, norm_gain, w_in, w_out):
    xf = tokens.astype(jnp.float32)
    scale = lax.rsqrt(jnp.mean(xf * xf, axis=-1, keepdims=True) + EPS)
    normed = (xf * scale * norm_gain).astype(jnp.bfloat16)
    whole_in = lax.all_gather(w_in, "fs", axis=0, tiled=True)
    pre = jnp.dot(collect(normed, "tp", 0), whole_in, preferred_element_type=jnp.float32)
    hidden = jnp.square(jax.nn.relu(pre)).astype(jnp.bfloat16)
    whole_out = lax.all_gather(w_out, "fs", axis=1, tiled=True)
    summed = lax.psum_scatter(
        jnp.dot(hidden, whole_out, preferred_element_type=jnp.float32).astype(jnp.bfloat16),
        "tp",
        scatter_dimension=0,
        tiled=True,
    ).astype(jnp.float32)
    return (xf + summed).astype(jnp.bfloat16)


def solution(mesh):
    in_specs = (P(("grp", "fs", "tp"), None), P(), P("fs", "tp"), P("tp", "fs"))
    out_specs = P(("grp", "fs", "tp"), None)
    return jax.shard_map(local, mesh=mesh, in_specs=in_specs, out_specs=out_specs, check_vma=False)
```

profile of v0, /device:TPU:40, one launch (start us, length us, event | category | flops | bytes accessed | tf_op | source)
XLA Modules:
  0.0 253.1 jit_solution(16195759570042781914)
XLA Ops:
  6.5 0.0 all-gather.3.cloned.1.call-start
  6.6 0.7 all-gather.3.cloned.1.call-update
  7.3 0.1 all-gather.5.cloned.1.call-start
  7.4 0.7 all-gather.5.cloned.1.call-update
  8.1 0.1 reduce-scatter.2.cloned.1.call-start
  8.2 1.2 fusion
  9.4 1.2 fusion.2
  10.7 0.5 broadcast_in_dim.2
  11.2 54.2 %all_to_all.5 = bf16[8,128,2048]{2,1,0:T(8,128)(2,1)} all-to-all(bf16[8,128,2048]{2,1,0:T(8,128)(2,1)S(1)} %broadcast_in_dim.2), channel_id=1, replica_groups=mesh['grp'=2,'fs'=16,'tp'=8] {'tp'}, dimensions={0} | all-to-all | bytes 8388608 | tf_op jit(solution)/shard_map/all_to_all | solution.py:11
  65.4 33.0 %all-gather.3.cloned.1.call-done = bf16[2048,1024]{1,0:T(8,128)(2,1)} async-done(((bf16[128,1024]{1,0:T(8,128)(2,1)}), bf16[2048,1024]{1,0:T(8,128)(2,1)}) %all-gather.3.cloned.1.call-update) | async-done | bytes 4194320 | tf_op jit(solution)/shard_map/all_gather | solution.py:29
  98.3 91.3 %all-gather.5.cloned.1.call-done = bf16[1024,2048]{1,0:T(8,128)(2,1)} async-done(((bf16[1024,128]{1,0:T(8,128)(2,1)}), bf16[1024,2048]{1,0:T(8,128)(2,1)}) %all-gather.5.cloned.1.call-update) | async-done | bytes 4194320 | tf_op jit(solution)/shard_map/all_gather | solution.py:32
  189.6 14.4 %convolution_convert_fusion = bf16[1024,2048]{1,0:T(8,128)(2,1)} fusion(bf16[1024,2048]{1,0:T(8,128)(2,1)} %all-gather.5.cloned.1.call-done, bf16[1024,2048]{1,0:T(8,128)(2,1)} %bitcast.4, bf16[2048,1024]{1,0:T(8,128)(2,1)} %all-gather.3.cloned.1.call-done), kind=kOutput, calls=%fused_computation.1 | convolution fusion | flops 8595177472 | bytes 16777216 | tf_op jit(solution)/shard_map/dot_general | solution.py:34
  204.0 0.0 copy-start
  204.0 0.1 reduce-scatter.2.cloned.1.call-update
  204.1 40.5 %reduce-scatter.2.cloned.1.call-done = bf16[128,2048]{1,0:T(8,128)(2,1)} async-done(((bf16[1024,2048]{1,0:T(8,128)(2,1)}), bf16[128,2048]{1,0:T(8,128)(2,1)}) %reduce-scatter.2.cloned.1.call-update) | async-done | bytes 524304 | tf_op jit(solution)/shard_map/reduce_scatter | solution.py:33
  244.5 0.0 copy-done
  244.5 2.0 fusion.3
  (1 shorter events, 0.0 us)
Async XLA Ops:
  6.5 91.8 %all-gather.3.cloned.1.call-start = ((), (), s32[]{:S(2)}) async-start(), calls=%async_computation.2 | async-start | bytes 4456448 | tf_op jit(solution)/shard_map/all_gather | solution.py:29
  7.3 182.3 %all-gather.5.cloned.1.call-start = ((), (), s32[]{:S(2)}) async-start(), calls=%async_computation.3 | async-start | bytes 4456448 | tf_op jit(solution)/shard_map/all_gather | solution.py:32
  8.1 236.4 %reduce-scatter.2.cloned.1.call-start = ((), (), s32[]{:S(2)}) async-start(), calls=%async_computation.4 | async-start | bytes 4718592 | tf_op jit(solution)/shard_map/reduce_scatter | solution.py:33
  204.0 40.6 %copy-start = (bf16[128,2048]{1,0:T(8,128)(2,1)S(1)}, bf16[128,2048]{1,0:T(8,128)(2,1)}, u32[]{:S(2)}) copy-start(bf16[128,2048]{1,0:T(8,128)(2,1)} %param.4) | copy-start | bytes 1572868
Sparse Core Ops, SparseCore 0:
  9.1 89.1 all-gather.2
  100.1 89.5 all-gather.4
  204.2 40.3 reduce-scatter.1
where the time goes:
time: 253 us
  waiting for transfers between devices  166 us (66%)
  blocking collectives  54.2 us (21%)
  matrix products  14.4 us (6%)
  between operations  13.1 us (5%)
  other arithmetic  4.44 us (2%)
    all_gather x1, waiting for transfers between devices, local(): whole_out = lax.all_gather(w_out, 'fs', axis=1, tiled=True)  91.3 us
    all_to_all x1, blocking collectives, from_everyone(): return lax.all_to_all(copies, axis, split_axis=0, concat_axis=0, tiled=True)  54.2 us
    reduce_scatter x1, waiting for transfers between devices, local(): lax.psum_scatter(jnp.dot(hidden, whole_out, preferred_element_type=jnp.fl...  40.5 us
    all_gather x1, waiting for transfers between devices, local(): whole_in = lax.all_gather(w_in, 'fs', axis=0, tiled=True)  33 us
    dot_general x1, matrix products, local(): jnp.dot(hidden, whole_out, preferred_element_type=jnp.float32)  14.4 us
  transfers between devices with their start and end apart: 3, of which 3 were waited for; matrix products, arithmetic and copies ran while one was open for 1% of the time, Pallas kernels for 0%

commit v1 on v0

--- a/solution.py
+++ b/solution.py
@@ -4,6 +4,28 @@
 from jax.sharding import PartitionSpec as P
 
 EPS = 1e-06
+
+
+def laid_out(parts, dim):
+    parts = jnp.moveaxis(parts, 0, dim)
+    shape = parts.shape
+    return parts.reshape(*shape[:dim], shape[dim] * shape[dim + 1], *shape[dim + 2 :])
+
+
+def collect_2(x, axis, dim):
+    devices = lax.axis_size(axis)
+    pairs = [(i, (i + 1) % devices) for i in range(devices)]
+    back = [(b, a) for a, b in pairs]
+    lower, upper = ([], [])
+    for step in range(devices - 1):
+        if step % 2 == 0:
+            lower.append(lax.ppermute(lower[-1] if lower else x, axis, pairs))
+        else:
+            upper.append(lax.ppermute(upper[-1] if upper else x, axis, back))
+    pieces = jnp.stack([*lower[::-1], x, *upper])
+    shift = lax.axis_index(axis) - len(lower)
+    pieces = pieces[(jnp.arange(devices) - shift) % devices]
+    return laid_out(pieces, dim)
 
 
 def from_everyone(shard, axis):
@@ -26,7 +48,7 @@
     xf = tokens.astype(jnp.float32)
     scale = lax.rsqrt(jnp.mean(xf * xf, axis=-1, keepdims=True) + EPS)
     normed = (xf * scale * norm_gain).astype(jnp.bfloat16)
-    whole_in = lax.all_gather(w_in, "fs", axis=0, tiled=True)
+    whole_in = collect_2(w_in, "fs", 0)
     pre = jnp.dot(collect(normed, "tp", 0), whole_in, preferred_element_type=jnp.float32)
     hidden = jnp.square(jax.nn.relu(pre)).astype(jnp.bfloat16)
     whole_out = lax.all_gather(w_out, "fs", axis=1, tiled=True)

time: 253 us -> 228 us (0.901)
  blocking collectives: 54.2 us -> 0 us
  starting transfers between devices: 0.13 us -> 35 us
  waiting for transfers between devices: 166 us -> 139 us
  local copies, waits for them, and re-layouts: 0.52 us -> 20.9 us
    all_gather x1, waiting for transfers between devices: 91.3 us -> 0.01 us  [local(): whole_out = lax.all_gather(w_out, 'fs', axis=1, tiled=True)]
    ppermute x0 -> x15, waiting for transfers between devices: none -> 66.9 us  [the longest x8 66.5 us: collect_2(): lower.append(lax.ppermute(lower[-1] if lower else x, axis, pairs))]
    all_to_all x1 -> x0, blocking collectives: 54.2 us -> none  [from_everyone(): return lax.all_to_all(copies, axis, split_axis=0, concat_axis=0, tiled=True)]
    all_gather x1 -> x0, waiting for transfers between devices: 33 us -> none  [local(): whole_in = lax.all_gather(w_in, 'fs', axis=0, tiled=True)]
    ppermute x0 -> x15, starting transfers between devices: none -> 30.1 us  [the longest x7 20.3 us: collect_2(): upper.append(lax.ppermute(upper[-1] if upper else x, axis, back))]
    all_to_all x0 -> x1, waiting for transfers between devices: none -> 28 us  [from_everyone(): return lax.all_to_all(copies, axis, split_axis=0, concat_axis=0, tiled=True)]
    unnamed x2 -> x19, local copies, waits for them, and re-layouts: 0.01 us -> 12.7 us
    gather x0 -> x1, local copies, waits for them, and re-layouts: none -> 4.94 us  [collect_2(): pieces = pieces[(jnp.arange(devices) - shift) % devices]]
  transfers between devices with their start and end apart: 3 -> 18, of which waited for: 3 -> 11; matrix products, arithmetic and copies ran while one was open for 1% -> 10% of each run, Pallas kernels for 0% -> 0%
where the time goes in v1:
time: 228 us; the launch traced here: 227 us
  waiting for transfers between devices  139 us (61%)
  starting transfers between devices  35 us (15%)
  local copies, waits for them, and re-layouts  20.9 us (9%)
  matrix products  14.4 us (6%)
  between operations  13.5 us (6%)
  other arithmetic  4.45 us (2%)
    ppermute x8, waiting for transfers between devices, collect_2(): lower.append(lax.ppermute(lower[-1] if lower else x, axis, pairs))  66.5 us
    reduce_scatter x1, waiting for transfers between devices, local(): lax.psum_scatter(jnp.dot(hidden, whole_out, preferred_element_type=jnp.fl...  43.1 us
    all_to_all x1, waiting for transfers between devices, from_everyone(): return lax.all_to_all(copies, axis, split_axis=0, concat_axis=0, tiled=True)  28 us
    ppermute x7, starting transfers between devices, collect_2(): upper.append(lax.ppermute(upper[-1] if upper else x, axis, back))  20.3 us
    dot_general x1, matrix products, local(): jnp.dot(hidden, whole_out, preferred_element_type=jnp.float32)  14.4 us
    unnamed x19, local copies, waits for them, and re-layouts  12.7 us
    ppermute x8, starting transfers between devices, collect_2(): lower.append(lax.ppermute(lower[-1] if lower else x, axis, pairs))  9.81 us
    gather x1, local copies, waits for them, and re-layouts, collect_2(): pieces = pieces[(jnp.arange(devices) - shift) % devices]  4.94 us
  transfers between devices with their start and end apart: 18, of which 11 were waited for; matrix products, arithmetic and copies ran while one was open for 10% of the time, Pallas kernels for 0%

profile of v1, /device:TPU:40, one launch (start us, length us, event | category | flops | bytes accessed | tf_op | source)
XLA Modules:
  0.0 227.1 jit_solution(6045182194048862733)
XLA Ops:
  7.3 2.9 %collective-permute-start = (bf16[128,1024]{1,0:T(8,128)(2,1)}, bf16[128,1024]{1,0:T(8,128)(2,1)S(1)}, u32[]{:S(2)}, u32[]{:S(2)}) collective-permute-start(bf16[128,1024]{1,0:T(8,128)(2,1)} %param.6), channel_id=1, source_target_pairs={{0,8},{8,16},{16,24},{24,32},{32,40},{40,48},{48,56},{56,64},{64,7... | collective-permute-start | bytes 786440 | tf_op jit(solution)/shard_map/ppermute | solution.py:22
  10.2 26.2 %collective-permute-done = bf16[128,1024]{1,0:T(8,128)(2,1)S(1)} collective-permute-done((bf16[128,1024]{1,0:T(8,128)(2,1)}, bf16[128,1024]{1,0:T(8,128)(2,1)S(1)}, u32[]{:S(2)}, u32[]{:S(2)}) %collective-permute-start) | collective-permute-done | bytes 262176 | tf_op jit(solution)/shard_map/ppermute | solution.py:22
  36.4 3.2 %collective-permute-start.8 = (bf16[128,1024]{1,0:T(8,128)(2,1)}, bf16[128,1024]{1,0:T(8,128)(2,1)S(1)}, u32[]{:S(2)}, u32[]{:S(2)}) collective-permute-start(bf16[128,1024]{1,0:T(8,128)(2,1)} %param.6), channel_id=1, source_target_pairs={{8,0},{16,8},{24,16},{32,24},{40,32},{48,40},{56,48},{64,56},{72,6... | collective-permute-start | bytes 786440 | tf_op jit(solution)/shard_map/ppermute | solution.py:24
  39.6 8.3 %collective-permute-done.1 = bf16[128,1024]{1,0:T(8,128)(2,1)S(1)} collective-permute-done((bf16[128,1024]{1,0:T(8,128)(2,1)S(1)}, bf16[128,1024]{1,0:T(8,128)(2,1)S(1)}, u32[]{:S(2)}, u32[]{:S(2)}) %collective-permute-start.1) | collective-permute-done | bytes 262176 | tf_op jit(solution)/shard_map/ppermute | solution.py:22
  48.2 3.0 %collective-permute-start.9 = (bf16[128,1024]{1,0:T(8,128)(2,1)S(1)}, bf16[128,1024]{1,0:T(8,128)(2,1)S(1)}, u32[]{:S(2)}, u32[]{:S(2)}) collective-permute-start(bf16[128,1024]{1,0:T(8,128)(2,1)S(1)} %collective-permute-done.8), channel_id=1, source_target_pairs={{8,0},{16,8},{24,16},{32,24},{40,32},{48,40},{56,48},{64,56},{72,6... | collective-permute-start | bytes 786440 | tf_op jit(solution)/shard_map/ppermute | solution.py:24
  51.2 7.9 %collective-permute-done.2 = bf16[128,1024]{1,0:T(8,128)(2,1)S(1)} collective-permute-done((bf16[128,1024]{1,0:T(8,128)(2,1)S(1)}, bf16[128,1024]{1,0:T(8,128)(2,1)S(1)}, u32[]{:S(2)}, u32[]{:S(2)}) %collective-permute-start.2) | collective-permute-done | bytes 262176 | tf_op jit(solution)/shard_map/ppermute | solution.py:22
  62.4 6.7 %collective-permute-done.3 = bf16[128,1024]{1,0:T(8,128)(2,1)S(1)} collective-permute-done((bf16[128,1024]{1,0:T(8,128)(2,1)S(1)}, bf16[128,1024]{1,0:T(8,128)(2,1)S(1)}, u32[]{:S(2)}, u32[]{:S(2)}) %collective-permute-start.3) | collective-permute-done | bytes 262176 | tf_op jit(solution)/shard_map/ppermute | solution.py:22
  69.1 2.0 collective-permute-start.4
  71.2 3.7 %collective-permute-start.11 = (bf16[128,1024]{1,0:T(8,128)(2,1)S(1)}, bf16[128,1024]{1,0:T(8,128)(2,1)S(1)}, u32[]{:S(2)}, u32[]{:S(2)}) collective-permute-start(bf16[128,1024]{1,0:T(8,128)(2,1)S(1)} %collective-permute-done.10), channel_id=1, source_target_pairs={{8,0},{16,8},{24,16},{32,24},{40,32},{48,40},{56,48},{64,56},{72,6... | collective-permute-start | bytes 786440 | tf_op jit(solution)/shard_map/ppermute | solution.py:24
  74.9 4.3 %collective-permute-done.4 = bf16[128,1024]{1,0:T(8,128)(2,1)S(1)} collective-permute-done((bf16[128,1024]{1,0:T(8,128)(2,1)S(1)}, bf16[128,1024]{1,0:T(8,128)(2,1)S(1)}, u32[]{:S(2)}, u32[]{:S(2)}) %collective-permute-start.4) | collective-permute-done | bytes 262176 | tf_op jit(solution)/shard_map/ppermute | solution.py:22
  79.2 2.5 %collective-permute-start.5 = (bf16[128,1024]{1,0:T(8,128)(2,1)S(1)}, bf16[128,1024]{1,0:T(8,128)(2,1)S(1)}, u32[]{:S(2)}, u32[]{:S(2)}) collective-permute-start(bf16[128,1024]{1,0:T(8,128)(2,1)S(1)} %collective-permute-done.4), channel_id=1, source_target_pairs={{0,8},{8,16},{16,24},{24,32},{32,40},{40,48},{48,56},{56,64},{64,7... | collective-permute-start | bytes 786440 | tf_op jit(solution)/shard_map/ppermute | solution.py:22
  81.7 3.0 %collective-permute-start.12 = (bf16[128,1024]{1,0:T(8,128)(2,1)S(1)}, bf16[128,1024]{1,0:T(8,128)(2,1)S(1)}, u32[]{:S(2)}, u32[]{:S(2)}) collective-permute-start(bf16[128,1024]{1,0:T(8,128)(2,1)S(1)} %collective-permute-done.11), channel_id=1, source_target_pairs={{8,0},{16,8},{24,16},{32,24},{40,32},{48,40},{56,48},{64,56},{72,6... | collective-permute-start | bytes 786440 | tf_op jit(solution)/shard_map/ppermute | solution.py:24
  84.7 5.8 %collective-permute-done.5 = bf16[128,1024]{1,0:T(8,128)(2,1)S(1)} collective-permute-done((bf16[128,1024]{1,0:T(8,128)(2,1)S(1)}, bf16[128,1024]{1,0:T(8,128)(2,1)S(1)}, u32[]{:S(2)}, u32[]{:S(2)}) %collective-permute-start.5) | collective-permute-done | bytes 262176 | tf_op jit(solution)/shard_map/ppermute | solution.py:22
  92.6 2.5 %collective-permute-start.13 = (bf16[128,1024]{1,0:T(8,128)(2,1)S(1)}, bf16[128,1024]{1,0:T(8,128)(2,1)S(1)}, u32[]{:S(2)}, u32[]{:S(2)}) collective-permute-start(bf16[128,1024]{1,0:T(8,128)(2,1)S(1)} %collective-permute-done.12), channel_id=1, source_target_pairs={{8,0},{16,8},{24,16},{32,24},{40,32},{48,40},{56,48},{64,56},{72,6... | collective-permute-start | bytes 786440 | tf_op jit(solution)/shard_map/ppermute | solution.py:24
  95.1 7.2 %collective-permute-done.6 = bf16[128,1024]{1,0:T(8,128)(2,1)} collective-permute-done((bf16[128,1024]{1,0:T(8,128)(2,1)S(1)}, bf16[128,1024]{1,0:T(8,128)(2,1)}, u32[]{:S(2)}, u32[]{:S(2)}) %collective-permute-start.6) | collective-permute-done | bytes 262176 | tf_op jit(solution)/shard_map/ppermute | solution.py:22
  103.6 2.5 %broadcast_in_dim.2 = bf16[8,128,2048]{2,1,0:T(8,128)(2,1)} broadcast(bf16[128,2048]{1,0:T(8,128)(2,1)S(1)} %fusion.2), dimensions={1,2} | broadcast | bytes 4718592 | tf_op jit(solution)/shard_map/broadcast_in_dim | solution.py:32
  106.1 4.9 %all-to-all-start = ((bf16[8,128,2048]{2,1,0:T(8,128)(2,1)}), bf16[8,128,2048]{2,1,0:T(8,128)(2,1)}, u32[]{:S(2)}, u32[]{:S(2)}) async-start(bf16[8,128,2048]{2,1,0:T(8,128)(2,1)} %broadcast_in_dim.2), calls=%async_computation | async-start | bytes 8388608 | tf_op jit(solution)/shard_map/all_to_all | solution.py:33
  111.1 3.2 %collective-permute-start.14 = (bf16[128,1024]{1,0:T(8,128)(2,1)S(1)}, bf16[128,1024]{1,0:T(8,128)(2,1)S(1)}, u32[]{:S(2)}, u32[]{:S(2)}) collective-permute-start(bf16[128,1024]{1,0:T(8,128)(2,1)S(1)} %collective-permute-done.13), channel_id=1, source_target_pairs={{8,0},{16,8},{24,16},{32,24},{40,32},{48,40},{56,48},{64,56},{72,6... | collective-permute-start | bytes 786440 | tf_op jit(solution)/shard_map/ppermute | solution.py:24
  114.3 1.7 bitcast_dynamic-update-slice_fusion.15
  127.8 4.9 %gather_fusion = bf16[16,128,1024]{2,1,0:T(8,128)(2,1)} fusion(bf16[16,128,1024]{2,1,0:T(8,128)(2,1)} %bitcast_dynamic-update-slice_fusion, s32[1024]{0:T(1024)S(1)} %pad_clamp_fusion), kind=kCustom, calls=%fused_computation | custom fusion | bytes 8388672 | tf_op jit(solution)/shard_map/gather | solution.py:27
  132.7 28.0 %all-to-all-done = bf16[8,128,2048]{2,1,0:T(8,128)(2,1)} async-done(((bf16[8,128,2048]{2,1,0:T(8,128)(2,1)}), bf16[8,128,2048]{2,1,0:T(8,128)(2,1)}, u32[]{:S(2)}, u32[]{:S(2)}) %all-to-all-start) | async-done | bytes 4194336 | tf_op jit(solution)/shard_map/all_to_all | solution.py:33
  160.7 14.4 %convolution_convert_fusion = bf16[1024,2048]{1,0:T(8,128)(2,1)} fusion(bf16[1024,2048]{1,0:T(8,128)(2,1)} %all-gather.2.cloned.1.call-done, bf16[1024,2048]{1,0:T(8,128)(2,1)} %bitcast, bf16[2048,1024]{1,0:T(8,128)(2,1)} %bitcast.39), kind=kOutput, calls=%fused_computation.2 | convolution fusion | flops 8595177472 | bytes 16777216 | tf_op jit(solution)/shard_map/dot_general | solution.py:56
  175.2 43.1 %reduce-scatter.2.cloned.1.call-done = bf16[128,2048]{1,0:T(8,128)(2,1)} async-done(((bf16[1024,2048]{1,0:T(8,128)(2,1)}), bf16[128,2048]{1,0:T(8,128)(2,1)}) %reduce-scatter.2.cloned.1.call-update) | async-done | bytes 524304 | tf_op jit(solution)/shard_map/reduce_scatter | solution.py:55
  218.3 2.0 fusion.3
  (43 shorter events, 19.6 us)
Async XLA Ops:
  6.5 154.2 %all-gather.2.cloned.1.call-start = ((), (), s32[]{:S(2)}) async-start(), calls=%async_computation.2 | async-start | bytes 4456448 | tf_op jit(solution)/shard_map/all_gather | solution.py:54
  7.3 29.1 %collective-permute-start = (bf16[128,1024]{1,0:T(8,128)(2,1)}, bf16[128,1024]{1,0:T(8,128)(2,1)S(1)}, u32[]{:S(2)}, u32[]{:S(2)}) collective-permute-start(bf16[128,1024]{1,0:T(8,128)(2,1)} %param.6), channel_id=1, source_target_pairs={{0,8},{8,16},{16,24},{24,32},{32,40},{40,48},{48,56},{56,64},{64,7... | collective-permute-start | bytes 786440 | tf_op jit(solution)/shard_map/ppermute | solution.py:22
  36.4 11.6 %collective-permute-start.1 = (bf16[128,1024]{1,0:T(8,128)(2,1)S(1)}, bf16[128,1024]{1,0:T(8,128)(2,1)S(1)}, u32[]{:S(2)}, u32[]{:S(2)}) collective-permute-start(bf16[128,1024]{1,0:T(8,128)(2,1)S(1)} %collective-permute-done), channel_id=1, source_target_pairs={{0,8},{8,16},{16,24},{24,32},{32,40},{40,48},{48,56},{56,64},{64,7... | collective-permute-start | bytes 786440 | tf_op jit(solution)/shard_map/ppermute | solution.py:22
  36.4 11.8 %collective-permute-start.8 = (bf16[128,1024]{1,0:T(8,128)(2,1)}, bf16[128,1024]{1,0:T(8,128)(2,1)S(1)}, u32[]{:S(2)}, u32[]{:S(2)}) collective-permute-start(bf16[128,1024]{1,0:T(8,128)(2,1)} %param.6), channel_id=1, source_target_pairs={{8,0},{16,8},{24,16},{32,24},{40,32},{48,40},{56,48},{64,56},{72,6... | collective-permute-start | bytes 786440 | tf_op jit(solution)/shard_map/ppermute | solution.py:24
  48.0 11.2 %collective-permute-start.2 = (bf16[128,1024]{1,0:T(8,128)(2,1)S(1)}, bf16[128,1024]{1,0:T(8,128)(2,1)S(1)}, u32[]{:S(2)}, u32[]{:S(2)}) collective-permute-start(bf16[128,1024]{1,0:T(8,128)(2,1)S(1)} %collective-permute-done.1), channel_id=1, source_target_pairs={{0,8},{8,16},{16,24},{24,32},{32,40},{40,48},{48,56},{56,64},{64,7... | collective-permute-start | bytes 786440 | tf_op jit(solution)/shard_map/ppermute | solution.py:22
  48.2 12.5 %collective-permute-start.9 = (bf16[128,1024]{1,0:T(8,128)(2,1)S(1)}, bf16[128,1024]{1,0:T(8,128)(2,1)S(1)}, u32[]{:S(2)}, u32[]{:S(2)}) collective-permute-start(bf16[128,1024]{1,0:T(8,128)(2,1)S(1)} %collective-permute-done.8), channel_id=1, source_target_pairs={{8,0},{16,8},{24,16},{32,24},{40,32},{48,40},{56,48},{64,56},{72,6... | collective-permute-start | bytes 786440 | tf_op jit(solution)/shard_map/ppermute | solution.py:24
  59.1 10.0 %collective-permute-start.3 = (bf16[128,1024]{1,0:T(8,128)(2,1)S(1)}, bf16[128,1024]{1,0:T(8,128)(2,1)S(1)}, u32[]{:S(2)}, u32[]{:S(2)}) collective-permute-start(bf16[128,1024]{1,0:T(8,128)(2,1)S(1)} %collective-permute-done.2), channel_id=1, source_target_pairs={{0,8},{8,16},{16,24},{24,32},{32,40},{40,48},{48,56},{56,64},{64,7... | collective-permute-start | bytes 786440 | tf_op jit(solution)/shard_map/ppermute | solution.py:22
  60.7 10.5 %collective-permute-start.10 = (bf16[128,1024]{1,0:T(8,128)(2,1)S(1)}, bf16[128,1024]{1,0:T(8,128)(2,1)S(1)}, u32[]{:S(2)}, u32[]{:S(2)}) collective-permute-start(bf16[128,1024]{1,0:T(8,128)(2,1)S(1)} %collective-permute-done.9), channel_id=1, source_target_pairs={{8,0},{16,8},{24,16},{32,24},{40,32},{48,40},{56,48},{64,56},{72,6... | collective-permute-start | bytes 786440 | tf_op jit(solution)/shard_map/ppermute | solution.py:24
  69.1 10.1 %collective-permute-start.4 = (bf16[128,1024]{1,0:T(8,128)(2,1)S(1)}, bf16[128,1024]{1,0:T(8,128)(2,1)S(1)}, u32[]{:S(2)}, u32[]{:S(2)}) collective-permute-start(bf16[128,1024]{1,0:T(8,128)(2,1)S(1)} %collective-permute-done.3), channel_id=1, source_target_pairs={{0,8},{8,16},{16,24},{24,32},{32,40},{40,48},{48,56},{56,64},{64,7... | collective-permute-start | bytes 786440 | tf_op jit(solution)/shard_map/ppermute | solution.py:22
  71.2 10.5 %collective-permute-start.11 = (bf16[128,1024]{1,0:T(8,128)(2,1)S(1)}, bf16[128,1024]{1,0:T(8,128)(2,1)S(1)}, u32[]{:S(2)}, u32[]{:S(2)}) collective-permute-start(bf16[128,1024]{1,0:T(8,128)(2,1)S(1)} %collective-permute-done.10), channel_id=1, source_target_pairs={{8,0},{16,8},{24,16},{32,24},{40,32},{48,40},{56,48},{64,56},{72,6... | collective-permute-start | bytes 786440 | tf_op jit(solution)/shard_map/ppermute | solution.py:24
  79.2 11.3 %collective-permute-start.5 = (bf16[128,1024]{1,0:T(8,128)(2,1)S(1)}, bf16[128,1024]{1,0:T(8,128)(2,1)S(1)}, u32[]{:S(2)}, u32[]{:S(2)}) collective-permute-start(bf16[128,1024]{1,0:T(8,128)(2,1)S(1)} %collective-permute-done.4), channel_id=1, source_target_pairs={{0,8},{8,16},{16,24},{24,32},{32,40},{40,48},{48,56},{56,64},{64,7... | collective-permute-start | bytes 786440 | tf_op jit(solution)/shard_map/ppermute | solution.py:22
  81.7 10.8 %collective-permute-start.12 = (bf16[128,1024]{1,0:T(8,128)(2,1)S(1)}, bf16[128,1024]{1,0:T(8,128)(2,1)S(1)}, u32[]{:S(2)}, u32[]{:S(2)}) collective-permute-start(bf16[128,1024]{1,0:T(8,128)(2,1)S(1)} %collective-permute-done.11), channel_id=1, source_target_pairs={{8,0},{16,8},{24,16},{32,24},{40,32},{48,40},{56,48},{64,56},{72,6... | collective-permute-start | bytes 786440 | tf_op jit(solution)/shard_map/ppermute | solution.py:24
  90.5 11.8 %collective-permute-start.6 = (bf16[128,1024]{1,0:T(8,128)(2,1)S(1)}, bf16[128,1024]{1,0:T(8,128)(2,1)}, u32[]{:S(2)}, u32[]{:S(2)}) collective-permute-start(bf16[128,1024]{1,0:T(8,128)(2,1)S(1)} %collective-permute-done.5), channel_id=1, source_target_pairs={{0,8},{8,16},{16,24},{24,32},{32,40},{40,48},{48,56},{56,64},{64,7... | collective-permute-start | bytes 786440 | tf_op jit(solution)/shard_map/ppermute | solution.py:22
  92.6 18.5 %collective-permute-start.13 = (bf16[128,1024]{1,0:T(8,128)(2,1)S(1)}, bf16[128,1024]{1,0:T(8,128)(2,1)S(1)}, u32[]{:S(2)}, u32[]{:S(2)}) collective-permute-start(bf16[128,1024]{1,0:T(8,128)(2,1)S(1)} %collective-permute-done.12), channel_id=1, source_target_pairs={{8,0},{16,8},{24,16},{32,24},{40,32},{48,40},{56,48},{64,56},{72,6... | collective-permute-start | bytes 786440 | tf_op jit(solution)/shard_map/ppermute | solution.py:24
  102.3 12.0 %collective-permute-start.7 = (bf16[128,1024]{1,0:T(8,128)(2,1)}, bf16[128,1024]{1,0:T(8,128)(2,1)}, u32[]{:S(2)}, u32[]{:S(2)}) collective-permute-start(bf16[128,1024]{1,0:T(8,128)(2,1)} %collective-permute-done.6), channel_id=1, source_target_pairs={{0,8},{8,16},{16,24},{24,32},{32,40},{40,48},{48,56},{56,64},{64,7... | collective-permute-start | bytes 786440 | tf_op jit(solution)/shard_map/ppermute | solution.py:22
  106.1 54.6 %all-to-all-start = ((bf16[8,128,2048]{2,1,0:T(8,128)(2,1)}), bf16[8,128,2048]{2,1,0:T(8,128)(2,1)}, u32[]{:S(2)}, u32[]{:S(2)}) async-start(bf16[8,128,2048]{2,1,0:T(8,128)(2,1)} %broadcast_in_dim.2), calls=%async_computation | async-start | bytes 8388608 | tf_op jit(solution)/shard_map/all_to_all | solution.py:33
  111.0 11.0 %copy-start.1 = (bf16[128,1024]{1,0:T(8,128)(2,1)S(1)}, bf16[128,1024]{1,0:T(8,128)(2,1)}, u32[]{:S(2)}) copy-start(bf16[128,1024]{1,0:T(8,128)(2,1)} %param.6) | copy-start | bytes 786436
  111.0 107.3 %reduce-scatter.2.cloned.1.call-start = ((), (), s32[]{:S(2)}) async-start(), calls=%async_computation.3 | async-start | bytes 4718592 | tf_op jit(solution)/shard_map/reduce_scatter | solution.py:55
  111.1 15.9 %collective-permute-start.14 = (bf16[128,1024]{1,0:T(8,128)(2,1)S(1)}, bf16[128,1024]{1,0:T(8,128)(2,1)S(1)}, u32[]{:S(2)}, u32[]{:S(2)}) collective-permute-start(bf16[128,1024]{1,0:T(8,128)(2,1)S(1)} %collective-permute-done.13), channel_id=1, source_target_pairs={{8,0},{16,8},{24,16},{32,24},{40,32},{48,40},{56,48},{64,56},{72,6... | collective-permute-start | bytes 786440 | tf_op jit(solution)/shard_map/ppermute | solution.py:24
  175.1 43.2 %copy-start = (bf16[128,2048]{1,0:T(8,128)(2,1)S(1)}, bf16[128,2048]{1,0:T(8,128)(2,1)}, u32[]{:S(2)}) copy-start(bf16[128,2048]{1,0:T(8,128)(2,1)} %param.4) | copy-start | bytes 1572868
Sparse Core Ops, SparseCore 0:
  9.1 125.3 all-gather.1
  175.3 42.9 reduce-scatter.1
